TPU v7x, 32 devices: a whole 2x2x4 slice. The times are simulated.
32 devices in a mesh: ep: 4 (over y, x), tp: 8 (over z, core).
Axes of the slice: x: 2, y: 2, z: 4, core: 2. Of those that a mesh axis runs over, the one named last changes fastest.
Arguments:
- features: bfloat16 [64, 1024], P('ep', 'tp'), may hold values from -6 to 6
- key_table: bfloat16 [65536, 1024], P('ep', 'tp'), may hold values from -0.1875 to 0.1875
- value_table: bfloat16 [65536, 1024], P('ep', 'tp'), may hold values from -6 to 6
- chosen: int32 [64, 4, 16], P('ep'), may hold values from 0 to 65535
- scores: float32 [64, 4, 16], P('ep'), may hold values from -8 to 8
Outputs:
- mixed: bfloat16 [64, 1024], P('ep', 'tp')
Inputs may be any that keep to these rules, and one draw needn't show every extreme that they name: Every chosen row is a row of the tables, 0 to 65535; rows may repeat, and a few rows are far more popular than the rest.
All inputs are finite; a program needn't handle non-finite values.
Results may differ from a plain program's by a relative error of at most 0.0065.
Values may be sent and summed in bfloat16 or wider, within the bound.
A program may use at most 64 MiB of HBM per device.

v0:
```python
import jax
import jax.numpy as jnp
from jax import lax
from jax.sharding import PartitionSpec as P


def in_blocks(func, arrays):
    total = arrays[0].shape[0]
    width = 32 if total % 32 == 0 else total
    count = total // width
    if count == 1:
        return func(arrays)
    shaped = tuple((item.reshape((count, width) + item.shape[1:]) for item in arrays))
    result = lax.map(func, shaped)
    return result.reshape((total,) + result.shape[2:])


def shards(features, key_table, value_table, chosen, scores):
    table_rows = key_table.shape[0]
    head_count = chosen.shape[1]
    top_count = chosen.shape[2]
    first_row = lax.axis_index("ep") * table_rows
    gate_weights = jax.nn.softmax(scores, axis=-1)
    chosen_all = lax.all_gather(chosen, "ep", axis=0, tiled=True)
    gates_all = lax.all_gather(gate_weights, "ep", axis=0, tiled=True)
    shifted = chosen_all - first_row
    owned_mask = (shifted >= 0) & (shifted < table_rows)
    local_rows = jnp.clip(shifted, 0, table_rows - 1).reshape(shifted.shape[0], -1)

    def dots_block(pair):
        token_block, picked = pair
        dense = lax.dot_general(
            token_block, key_table, (((1,), (1,)), ((), ())), preferred_element_type=jnp.float32
        )
        return jnp.take_along_axis(dense, picked, axis=1)

    def partial_dots(token_block):
        row_count = token_block.shape[0]
        picked = lax.slice_in_dim(local_rows, 0, row_count, axis=0)
        keep_mask = lax.slice_in_dim(owned_mask, 0, row_count, axis=0)
        products = in_blocks(dots_block, (token_block, picked))
        return jnp.where(keep_mask.reshape(row_count, -1), products, 0.0)

    partial_value = partial_dots(lax.all_gather(features, "ep", axis=0, tiled=True))
    partial_value = partial_value.reshape(-1, head_count, top_count)
    products = lax.psum(partial_value, "tp")
    row_weights = (gates_all * jax.nn.gelu(products, approximate=False)).astype(jnp.bfloat16)
    row_weights = jnp.where(owned_mask, row_weights, jnp.zeros_like(row_weights))
    flat_weights = row_weights.reshape(row_weights.shape[0], -1)

    def value_block(pair):
        block_weights, picked = pair
        width = picked.shape[0]
        token_ids = lax.broadcasted_iota(jnp.int32, picked.shape, 0)
        dense = (
            jnp.zeros((width, table_rows), jnp.float32)
            .at[token_ids, picked]
            .add(block_weights.astype(jnp.float32))
        )
        upper = dense.astype(jnp.bfloat16)
        lower = (dense - upper.astype(jnp.float32)).astype(jnp.bfloat16)
        summed = jnp.dot(upper, value_table, preferred_element_type=jnp.float32)
        return summed + jnp.dot(lower, value_table, preferred_element_type=jnp.float32)

    def owner_term(row_count):
        picked = lax.slice_in_dim(local_rows, 0, row_count, axis=0)
        block_weights = lax.slice_in_dim(flat_weights, 0, row_count, axis=0)
        return in_blocks(value_block, (block_weights, picked))

    summed = lax.psum_scatter(
        owner_term(lax.axis_size("ep") * features.shape[0]), "ep", scatter_dimension=0, tiled=True
    )
    return summed.astype(jnp.bfloat16)


def solution(mesh):
    return jax.shard_map(
        shards,
        mesh=mesh,
        in_specs=(
            P("ep", "tp"),
            P("ep", "tp"),
            P("ep", "tp"),
            P("ep", None, None),
            P("ep", None, None),
        ),
        out_specs=P("ep", "tp"),
        check_vma=False,
    )
```

profile of v0, /device:TPU:0, one launch (start us, length us, event | category | flops | bytes accessed | tf_op | source)
XLA Modules:
  0.0 150.6 jit_solution(2925781054300284029)
XLA Ops:
  0.0 10.1 %all_gather.9 = s32[64,4,16]{2,1,0:T(4,128)S(1)} all-gather(s32[16,4,16]{2,1,0:T(4,128)} %param.12), channel_id=1, replica_groups=mesh['ep'=4,'tp'=8] {'ep'}, dimensions={0}, use_global_device_ids=true | all-gather | bytes 20480 | tf_op jit(solution)/shard_map/all_gather | solution.py:24
  10.1 0.1 copy.12
  10.2 0.1 reshape_reshape.7
  10.3 0.1 copy.16
  10.4 8.0 %all_gather.11 = bf16[64,128]{1,0:T(8,128)(2,1)S(1)} all-gather(bf16[16,128]{1,0:T(8,128)(2,1)} %param.9), channel_id=1, replica_groups=mesh['ep'=4,'tp'=8] {'ep'}, dimensions={0}, use_global_device_ids=true | all-gather | bytes 20480 | tf_op jit(solution)/shard_map/all_gather | solution.py:44
  18.4 0.0 copy-start.3
  18.4 0.0 copy-start.1
  18.4 0.0 copy-start.2
  18.4 41.2 %while.20 = (s32[]{:T(128)}, f32[2,32,64]{2,1,0:T(8,128)S(1)}, s32[2,32,64]{2,1,0:T(8,128)S(1)}, bf16[2,32,128]{2,1,0:T(8,128)(2,1)S(1)}, bf16[16384,128]{1,0:T(8,128)(2,1)}, /*index=5*/s32[]{:T(128)}) while((s32[]{:T(128)}, f32[2,32,64]{2,1,0:T(8,128)S(1)}, s32[2,32,64]{2,1,0:T(8,128)S(1)}, bf16[2,32,128]{2,1,0:T(8,128)(2,1)S(1)}, ...), condition=%wide.region_3.4_spmd, body=%wide.region_2.3_spmd.sunk | while | flops 134248448 | bytes 6430801 | solution.py:14
  18.4 3.7 %fusion.47 = f32[32,16384]{1,0:T(8,128)S(1)} fusion(bf16[16384,128]{1,0:T(8,128)(2,1)} %get-tuple-element.181, bf16[2,32,128]{2,1,0:T(8,128)(2,1)S(1)} %get-tuple-element.180, s32[]{:T(128)} %get-tuple-element.171), kind=kOutput, calls=%fused_computation.8.clone.1 | convolution fusion | flops 134217728 | bytes 6299652 | tf_op jit(solution)/shard_map/while/body/eval_jaxpr/dot_general | solution.py:32
  22.2 0.1 reshape.128
  22.2 16.6 %gather_fusion = f32[2048]{0:T(1024)S(1)} fusion(f32[32,16384]{1,0:T(8,128)S(1)} %fusion.47, s32[2048]{0:T(1024)S(1)} %reshape.128), kind=kCustom, calls=%fused_computation.clone.1 | custom fusion | bytes 32768 | tf_op jit(solution)/shard_map/while/body/eval_jaxpr/jit(take_along_axis)/gather | solution.py:35
  38.9 0.1 gather.11
  39.0 3.7 %fusion.47 = f32[32,16384]{1,0:T(8,128)S(1)} fusion(bf16[16384,128]{1,0:T(8,128)(2,1)} %get-tuple-element.181, bf16[2,32,128]{2,1,0:T(8,128)(2,1)S(1)} %get-tuple-element.180, s32[]{:T(128)} %get-tuple-element.171), kind=kOutput, calls=%fused_computation.8.clone.1 | convolution fusion | flops 134217728 | bytes 6299652 | tf_op jit(solution)/shard_map/while/body/eval_jaxpr/dot_general | solution.py:32
  42.7 0.1 reshape.128
  42.8 16.6 %gather_fusion = f32[2048]{0:T(1024)S(1)} fusion(f32[32,16384]{1,0:T(8,128)S(1)} %fusion.47, s32[2048]{0:T(1024)S(1)} %reshape.128), kind=kCustom, calls=%fused_computation.clone.1 | custom fusion | bytes 32768 | tf_op jit(solution)/shard_map/while/body/eval_jaxpr/jit(take_along_axis)/gather | solution.py:35
  59.5 0.1 gather.11
  59.6 0.1 copy.14
  59.6 0.1 reshape.94
  59.8 26.0 %psum.7 = f32[64,4,16]{0,2,1:T(8,128)S(1)} all-reduce(f32[64,4,16]{0,2,1:T(8,128)S(1)} %get-tuple-element.101), channel_id=1, replica_groups=mesh['ep'=4,'tp'=8] {'tp'}, use_global_device_ids=true, to_apply=%region_4.5 | all-reduce | flops 4096 | bytes 32768 | tf_op jit(solution)/shard_map/psum | solution.py:46
  85.8 0.0 copy-done.3
  85.8 0.2 fusion.17
  86.0 7.7 %all_gather.10 = f32[64,4,16]{2,1,0:T(4,128)S(1)} all-gather(f32[16,4,16]{2,1,0:T(4,128)S(1)} %fusion.17), channel_id=1, replica_groups=mesh['ep'=4,'tp'=8] {'ep'}, dimensions={0}, use_global_device_ids=true | all-gather | bytes 20480 | tf_op jit(solution)/shard_map/all_gather | solution.py:25
  93.6 0.1 copy.15
  93.7 0.1 fusion.30
  93.8 0.1 reshape_reshape.8
  93.9 0.1 copy.17
  94.0 0.0 copy-done.1
  94.0 0.0 copy-done.2
  94.0 0.0 copy-start.4
  94.0 39.5 %while.21 = (s32[]{:T(128)}, f32[2,32,128]{2,1,0:T(8,128)S(1)}, s32[2,32,64]{2,1,0:T(8,128)S(1)}, bf16[2,32,64]{2,1,0:T(8,128)(2,1)S(1)}, bf16[16384,128]{1,0:T(...) while((s32[]{:T(128)}, f32[2,32,128]{2,1,0:T(8,128)S(1)}, ...), condition=%wide.region_7.8_spmd, body=%wide.region_5.7_spmd.sunk | while | flops 271101952 | bytes 35831960 | solution.py:14
  94.1 0.1 multiply_reduce_fusion.2
  94.1 0.1 and_reduce_fusion.2
  94.2 0.1 reshape.131
  94.3 0.1 reshape.132
  94.4 13.3 %scatter_custom_fusion.5 = f32[524288]{0:T(1024)} fusion(s32[2048]{0:T(1024)S(1)} %reshape.131, f32[2048]{0:T(1024)S(1)} %reshape.132, f32[]{:T(128)} %constant.53.clone.1..sunk), kind=kCustom, calls=%fused_computation.16.clone.1 | custom fusion | flops 2048 | bytes 2097156 | tf_op jit(solution)/shard_map/while
  107.7 1.7 %reshape.133 = f32[32,16384]{1,0:T(8,128)S(1)} reshape(f32[524288]{0:T(1024)} %scatter_custom_fusion.5) | data formatting | bytes 4194304 | tf_op jit(solution)/shard_map/while/body/eval_jaxpr/scatter-add | solution.py:58
  109.5 0.0 copy-start
  109.5 3.1 %fusion.53 = f32[32,128]{1,0:T(8,128)S(1)} fusion(bf16[16384,128]{1,0:T(8,128)(2,1)} %get-tuple-element.205, f32[32,16384]{1,0:T(8,128)S(1)} %reshape.133), kind=kOutput, calls=%fused_computation.19.clone.1 | convolution fusion | flops 134742016 | bytes 6307840 | tf_op jit(solution)/shard_map/while/body/eval_jaxpr/dot_general | solution.py:62
  112.6 0.3 copy-done
  112.9 0.8 fusion.54
  113.8 0.1 multiply_reduce_fusion.2
  113.8 0.1 and_reduce_fusion.2
  113.9 0.1 reshape.131
  114.0 0.1 reshape.132
  114.1 13.5 %scatter_custom_fusion.5 = f32[524288]{0:T(1024)} fusion(s32[2048]{0:T(1024)S(1)} %reshape.131, f32[2048]{0:T(1024)S(1)} %reshape.132, f32[]{:T(128)} %constant.53.clone.1..sunk), kind=kCustom, calls=%fused_computation.16.clone.1 | custom fusion | flops 2048 | bytes 2097156 | tf_op jit(solution)/shard_map/while
  127.6 1.7 %reshape.133 = f32[32,16384]{1,0:T(8,128)S(1)} reshape(f32[524288]{0:T(1024)} %scatter_custom_fusion.5) | data formatting | bytes 4194304 | tf_op jit(solution)/shard_map/while/body/eval_jaxpr/scatter-add | solution.py:58
  129.3 0.0 copy-start
  129.3 3.1 %fusion.53 = f32[32,128]{1,0:T(8,128)S(1)} fusion(bf16[16384,128]{1,0:T(8,128)(2,1)} %get-tuple-element.205, f32[32,16384]{1,0:T(8,128)S(1)} %reshape.133), kind=kOutput, calls=%fused_computation.19.clone.1 | convolution fusion | flops 134742016 | bytes 6307840 | tf_op jit(solution)/shard_map/while/body/eval_jaxpr/dot_general | solution.py:62
  132.4 0.3 copy-done
  132.8 0.8 fusion.54
  133.6 15.1 %all-reduce = bf16[64,128]{1,0:T(8,128)(2,1)S(1)} all-reduce(f32[64,128]{1,0:T(8,128)S(1)} %bitcast.41), channel_id=2, replica_groups=mesh['ep'=4,'tp'=8] {'ep'}, use_global_device_ids=true, to_apply=%region_8.9.clone | all-reduce | flops 8192 | bytes 49152
  148.7 0.0 copy-done.4
  148.7 0.6 dynamic-slice
  150.0 0.6 dynamic-slice_convert_fusion.1
  (16 shorter events, 0.2 us)
Async XLA Ops:
  18.4 67.4 %copy-start.3 = (f32[16,4,16]{2,1,0:T(4,128)S(1)}, f32[16,4,16]{2,1,0:T(4,128)}, u32[]{:S(2)}) copy-start(f32[16,4,16]{2,1,0:T(4,128)} %param.13) | copy-start | bytes 12292
  18.4 75.6 %copy-start.1 = (s32[2]{0:T(128)S(1)}, s32[2]{0:T(128)}, u32[]{:S(2)}) copy-start(s32[2]{0:T(128)} %constant.199) | copy-start | bytes 28
  18.4 75.6 %copy-start.2 = (s32[2]{0:T(128)S(1)}, s32[2]{0:T(128)}, u32[]{:S(2)}) copy-start(s32[2]{0:T(128)} %constant.200) | copy-start | bytes 28
  94.0 54.7 %copy-start.4 = (u32[32]{0:T(128)S(1)}, u32[32]{0:T(128)}, u32[]{:S(2)}) copy-start(u32[32]{0:T(128)} %constant.148) | copy-start | bytes 388
  109.5 3.5 %copy-start = (bf16[16384,128]{1,0:T(8,128)(2,1)S(1)}, bf16[16384,128]{1,0:T(8,128)(2,1)}, u32[]{:S(2)}) copy-start(bf16[16384,128]{1,0:T(8,128)(2,1)} %get-tuple-element.205) | copy-start | bytes 12582916 | tf_op jit(solution)/shard_map/while
  129.3 3.5 %copy-start = (bf16[16384,128]{1,0:T(8,128)(2,1)S(1)}, bf16[16384,128]{1,0:T(8,128)(2,1)}, u32[]{:S(2)}) copy-start(bf16[16384,128]{1,0:T(8,128)(2,1)} %get-tuple-element.205) | copy-start | bytes 12582916 | tf_op jit(solution)/shard_map/while
where the time goes:
time: 151 us
  blocking collectives  66.9 us (44%)
  local copies, waits for them, and re-layouts  40 us (26%)
  other arithmetic  27.6 us (18%)
  matrix products  15.2 us (10%)
    gather x6, local copies, waits for them, and re-layouts, dots_block(): return jnp.take_along_axis(dense, picked, axis=1)  33.6 us
    while x8, other arithmetic  27.1 us
    psum x1, blocking collectives, shards(): products = lax.psum(partial_value, 'tp')  26 us
    unnamed x1, blocking collectives  15.1 us
    all_gather x1, blocking collectives, shards(): chosen_all = lax.all_gather(chosen, 'ep', axis=0, tiled=True)  10.1 us
    all_gather x1, blocking collectives, shards(): lax.all_gather(features, 'ep', axis=0, tiled=True)  7.96 us
    all_gather x1, blocking collectives, shards(): gates_all = lax.all_gather(gate_weights, 'ep', axis=0, tiled=True)  7.69 us
    dot_general x2, matrix products, dots_block(): lax.dot_general(token_block, key_table, (((1,), (1,)), ((), ())), preferr...  7.45 us

commit v1 on v0

--- a/solution.py
+++ b/solution.py
@@ -43,7 +43,9 @@
 
     partial_value = partial_dots(lax.all_gather(features, "ep", axis=0, tiled=True))
     partial_value = partial_value.reshape(-1, head_count, top_count)
-    products = lax.psum(partial_value, "tp")
+    products = partial_value
+    for hop in (1, 2, 4):
+        products = products + lax.ppermute(products, "tp", [(dev, dev ^ hop) for dev in range(8)])
     row_weights = (gates_all * jax.nn.gelu(products, approximate=False)).astype(jnp.bfloat16)
     row_weights = jnp.where(owned_mask, row_weights, jnp.zeros_like(row_weights))
     flat_weights = row_weights.reshape(row_weights.shape[0], -1)

time: 151 us -> 133 us (0.88)
  blocking collectives: 66.9 us -> 41.2 us
  starting transfers between devices: 0 us -> 4.23 us
  waiting for transfers between devices: 0 us -> 3.54 us
    psum x1 -> x0, blocking collectives: 26 us -> none  [shards(): products = lax.psum(partial_value, 'tp')]
    ppermute x0 -> x3, starting transfers between devices: none -> 4.23 us  [shards(): lax.ppermute(products, 'tp', [(dev, dev ^ hop) for dev in range(8)])]
    ppermute x0 -> x3, waiting for transfers between devices: none -> 3.54 us  [shards(): lax.ppermute(products, 'tp', [(dev, dev ^ hop) for dev in range(8)])]
  transfers between devices with their start and end apart: 0 -> 3, of which waited for: 0 -> 2; matrix products, arithmetic and copies ran while one was open for 0% -> 1% of each run, Pallas kernels for 0% -> 0%
where the time goes in v1:
time: 133 us
  blocking collectives  41.2 us (31%)
  local copies, waits for them, and re-layouts  40.1 us (30%)
  other arithmetic  27.6 us (21%)
  matrix products  15.2 us (11%)
  starting transfers between devices  4.23 us (3%)
  waiting for transfers between devices  3.54 us (3%)
    gather x6, local copies, waits for them, and re-layouts, dots_block(): return jnp.take_along_axis(dense, picked, axis=1)  33.6 us
    while x8, other arithmetic  27.1 us
    unnamed x1, blocking collectives  15.2 us
    all_gather x1, blocking collectives, shards(): chosen_all = lax.all_gather(chosen, 'ep', axis=0, tiled=True)  10.1 us
    all_gather x1, blocking collectives, shards(): lax.all_gather(features, 'ep', axis=0, tiled=True)  7.96 us
    all_gather x1, blocking collectives, shards(): gates_all = lax.all_gather(gate_weights, 'ep', axis=0, tiled=True)  7.86 us
    dot_general x2, matrix products, dots_block(): lax.dot_general(token_block, key_table, (((1,), (1,)), ((), ())), preferr...  7.46 us
    dot_general x2, matrix products, value_block(): summed = jnp.dot(upper, value_table, preferred_element_type=jnp.float32)  6.18 us
  transfers between devices with their start and end apart: 3, of which 2 were waited for; matrix products, arithmetic and copies ran while one was open for 1% of the time, Pallas kernels for 0%

profile of v1, /device:TPU:0, one launch (start us, length us, event | category | flops | bytes accessed | tf_op | source)
XLA Modules:
  0.0 132.8 jit_solution(15712404637451524408)
XLA Ops:
  0.0 10.1 %all_gather.9 = s32[64,4,16]{2,1,0:T(4,128)S(1)} all-gather(s32[16,4,16]{2,1,0:T(4,128)} %param.12), channel_id=1, replica_groups=mesh['ep'=4,'tp'=8] {'ep'}, dimensions={0}, use_global_device_ids=true | all-gather | bytes 20480 | tf_op jit(solution)/shard_map/all_gather | solution.py:24
  10.1 0.1 copy.12
  10.2 0.1 reshape_reshape.7
  10.3 0.1 copy.16
  10.4 8.0 %all_gather.11 = bf16[64,128]{1,0:T(8,128)(2,1)S(1)} all-gather(bf16[16,128]{1,0:T(8,128)(2,1)} %param.9), channel_id=1, replica_groups=mesh['ep'=4,'tp'=8] {'ep'}, dimensions={0}, use_global_device_ids=true | all-gather | bytes 20480 | tf_op jit(solution)/shard_map/all_gather | solution.py:44
  18.4 0.0 copy-start.3
  18.4 0.0 copy-start.4
  18.4 0.0 copy-start.1
  18.4 0.0 copy-start.2
  18.4 41.2 %while.20 = (s32[]{:T(128)}, f32[2,32,64]{2,1,0:T(8,128)S(1)}, s32[2,32,64]{2,1,0:T(8,128)S(1)}, bf16[2,32,128]{2,1,0:T(8,128)(2,1)S(1)}, bf16[16384,128]{1,0:T(8,128)(2,1)}, /*index=5*/s32[]{:T(128)}) while((s32[]{:T(128)}, f32[2,32,64]{2,1,0:T(8,128)S(1)}, s32[2,32,64]{2,1,0:T(8,128)S(1)}, bf16[2,32,128]{2,1,0:T(8,128)(2,1)S(1)}, ...), condition=%wide.region_3.4_spmd, body=%wide.region_2.3_spmd.sunk | while | flops 134248448 | bytes 6430801 | solution.py:14
  18.4 3.7 %fusion.47 = f32[32,16384]{1,0:T(8,128)S(1)} fusion(bf16[16384,128]{1,0:T(8,128)(2,1)} %get-tuple-element.181, bf16[2,32,128]{2,1,0:T(8,128)(2,1)S(1)} %get-tuple-element.180, s32[]{:T(128)} %get-tuple-element.171), kind=kOutput, calls=%fused_computation.8.clone.1 | convolution fusion | flops 134217728 | bytes 6299652 | tf_op jit(solution)/shard_map/while/body/eval_jaxpr/dot_general | solution.py:32
  22.2 0.1 reshape.128
  22.3 16.6 %gather_fusion = f32[2048]{0:T(1024)S(1)} fusion(f32[32,16384]{1,0:T(8,128)S(1)} %fusion.47, s32[2048]{0:T(1024)S(1)} %reshape.128), kind=kCustom, calls=%fused_computation.clone.1 | custom fusion | bytes 32768 | tf_op jit(solution)/shard_map/while/body/eval_jaxpr/jit(take_along_axis)/gather | solution.py:35
  38.9 0.1 gather.11
  39.0 3.7 %fusion.47 = f32[32,16384]{1,0:T(8,128)S(1)} fusion(bf16[16384,128]{1,0:T(8,128)(2,1)} %get-tuple-element.181, bf16[2,32,128]{2,1,0:T(8,128)(2,1)S(1)} %get-tuple-element.180, s32[]{:T(128)} %get-tuple-element.171), kind=kOutput, calls=%fused_computation.8.clone.1 | convolution fusion | flops 134217728 | bytes 6299652 | tf_op jit(solution)/shard_map/while/body/eval_jaxpr/dot_general | solution.py:32
  42.8 0.1 reshape.128
  42.8 16.6 %gather_fusion = f32[2048]{0:T(1024)S(1)} fusion(f32[32,16384]{1,0:T(8,128)S(1)} %fusion.47, s32[2048]{0:T(1024)S(1)} %reshape.128), kind=kCustom, calls=%fused_computation.clone.1 | custom fusion | bytes 32768 | tf_op jit(solution)/shard_map/while/body/eval_jaxpr/jit(take_along_axis)/gather | solution.py:35
  59.5 0.1 gather.11
  59.6 0.1 copy.14
  59.7 0.1 reshape.94
  59.8 0.1 collective-permute-start
  59.9 1.2 collective-permute-done
  61.1 1.6 %collective-permute-start.1 = (f32[64,4,16]{0,2,1:T(8,128)S(1)}, f32[64,4,16]{0,2,1:T(8,128)S(1)}, u32[]{:S(2)}, u32[]{:S(2)}) collective-permute-start(f32[64,4,16]{0,2,1:T(8,128)S(1)} %add.56), channel_id=1, source_target_pairs={{0,2},{1,3},{2,0},{3,1},{4,6},{5,7},{6,4},{7,5},{8,10},{9,11},{10,... | collective-permute-start | bytes 49160 | tf_op jit(solution)/shard_map/ppermute | solution.py:48
  62.6 2.3 %collective-permute-done.1 = f32[64,4,16]{0,2,1:T(8,128)S(1)} collective-permute-done((f32[64,4,16]{0,2,1:T(8,128)S(1)}, f32[64,4,16]{0,2,1:T(8,128)S(1)}, u32[]{:S(2)}, u32[]{:S(2)}) %collective-permute-start.1) | collective-permute-done | bytes 16416 | tf_op jit(solution)/shard_map/ppermute | solution.py:48
  65.0 2.6 %collective-permute-start.2 = (f32[64,4,16]{0,2,1:T(8,128)S(1)}, f32[64,4,16]{0,2,1:T(8,128)S(1)}, u32[]{:S(2)}, u32[]{:S(2)}) collective-permute-start(f32[64,4,16]{0,2,1:T(8,128)S(1)} %add.57), channel_id=1, source_target_pairs={{0,4},{1,5},{2,6},{3,7},{4,0},{5,1},{6,2},{7,3},{8,12},{9,13},{10,... | collective-permute-start | bytes 49160 | tf_op jit(solution)/shard_map/ppermute | solution.py:48
  67.6 0.0 copy-done.3
  67.6 0.2 fusion.17
  67.8 7.9 %all_gather.10 = f32[64,4,16]{2,1,0:T(4,128)S(1)} all-gather(f32[16,4,16]{2,1,0:T(4,128)S(1)} %fusion.17), channel_id=1, replica_groups=mesh['ep'=4,'tp'=8] {'ep'}, dimensions={0}, use_global_device_ids=true | all-gather | bytes 20480 | tf_op jit(solution)/shard_map/all_gather | solution.py:25
  75.6 0.1 copy.15
  75.7 0.0 copy-done.4
  75.7 0.7 dynamic-slice
  77.1 0.0 collective-permute-done.2
  77.1 0.1 fusion.30
  77.2 0.1 reshape_reshape.8
  77.3 0.1 copy.17
  77.4 0.0 copy-done.1
  77.4 0.0 copy-done.2
  77.4 39.5 %while.21 = (s32[]{:T(128)}, f32[2,32,128]{2,1,0:T(8,128)S(1)}, s32[2,32,64]{2,1,0:T(8,128)S(1)}, bf16[2,32,64]{2,1,0:T(8,128)(2,1)S(1)}, bf16[16384,128]{1,0:T(...) while((s32[]{:T(128)}, f32[2,32,128]{2,1,0:T(8,128)S(1)}, ...), condition=%wide.region_6.7_spmd, body=%wide.region_4.6_spmd.sunk | while | flops 271101952 | bytes 35831960 | solution.py:14
  77.4 0.1 multiply_reduce_fusion.2
  77.5 0.1 and_reduce_fusion.2
  77.6 0.1 reshape.131
  77.7 0.1 reshape.132
  77.8 13.3 %scatter_custom_fusion.5 = f32[524288]{0:T(1024)} fusion(s32[2048]{0:T(1024)S(1)} %reshape.131, f32[2048]{0:T(1024)S(1)} %reshape.132, f32[]{:T(128)} %constant.53.clone.1..sunk), kind=kCustom, calls=%fused_computation.16.clone.1 | custom fusion | flops 2048 | bytes 2097156 | tf_op jit(solution)/shard_map/while
  91.1 1.7 %reshape.133 = f32[32,16384]{1,0:T(8,128)S(1)} reshape(f32[524288]{0:T(1024)} %scatter_custom_fusion.5) | data formatting | bytes 4194304 | tf_op jit(solution)/shard_map/while/body/eval_jaxpr/scatter-add | solution.py:60
  92.8 0.0 copy-start
  92.9 3.1 %fusion.53 = f32[32,128]{1,0:T(8,128)S(1)} fusion(bf16[16384,128]{1,0:T(8,128)(2,1)} %get-tuple-element.205, f32[32,16384]{1,0:T(8,128)S(1)} %reshape.133), kind=kOutput, calls=%fused_computation.19.clone.1 | convolution fusion | flops 134742016 | bytes 6307840 | tf_op jit(solution)/shard_map/while/body/eval_jaxpr/dot_general | solution.py:64
  95.9 0.3 copy-done
  96.3 0.8 fusion.54
  97.1 0.1 multiply_reduce_fusion.2
  97.2 0.1 and_reduce_fusion.2
  97.3 0.1 reshape.131
  97.4 0.1 reshape.132
  97.4 13.5 %scatter_custom_fusion.5 = f32[524288]{0:T(1024)} fusion(s32[2048]{0:T(1024)S(1)} %reshape.131, f32[2048]{0:T(1024)S(1)} %reshape.132, f32[]{:T(128)} %constant.53.clone.1..sunk), kind=kCustom, calls=%fused_computation.16.clone.1 | custom fusion | flops 2048 | bytes 2097156 | tf_op jit(solution)/shard_map/while
  110.9 1.7 %reshape.133 = f32[32,16384]{1,0:T(8,128)S(1)} reshape(f32[524288]{0:T(1024)} %scatter_custom_fusion.5) | data formatting | bytes 4194304 | tf_op jit(solution)/shard_map/while/body/eval_jaxpr/scatter-add | solution.py:60
  112.7 0.0 copy-start
  112.7 3.1 %fusion.53 = f32[32,128]{1,0:T(8,128)S(1)} fusion(bf16[16384,128]{1,0:T(8,128)(2,1)} %get-tuple-element.205, f32[32,16384]{1,0:T(8,128)S(1)} %reshape.133), kind=kOutput, calls=%fused_computation.19.clone.1 | convolution fusion | flops 134742016 | bytes 6307840 | tf_op jit(solution)/shard_map/while/body/eval_jaxpr/dot_general | solution.py:64
  115.8 0.3 copy-done
  116.1 0.8 fusion.54
  116.9 15.2 %all-reduce = bf16[64,128]{1,0:T(8,128)(2,1)S(1)} all-reduce(f32[64,128]{1,0:T(8,128)S(1)} %bitcast.41), channel_id=2, replica_groups=mesh['ep'=4,'tp'=8] {'ep'}, use_global_device_ids=true, to_apply=%region_7.8.clone | all-reduce | flops 8192 | bytes 49152
  132.2 0.6 dynamic-slice_convert_fusion.1
  (18 shorter events, 0.2 us)
Async XLA Ops:
  18.4 49.2 %copy-start.3 = (f32[16,4,16]{2,1,0:T(4,128)S(1)}, f32[16,4,16]{2,1,0:T(4,128)}, u32[]{:S(2)}) copy-start(f32[16,4,16]{2,1,0:T(4,128)} %param.13) | copy-start | bytes 12292
  18.4 57.3 %copy-start.4 = (u32[32]{0:T(128)S(1)}, u32[32]{0:T(128)}, u32[]{:S(2)}) copy-start(u32[32]{0:T(128)} %constant.148) | copy-start | bytes 388
  18.4 59.0 %copy-start.1 = (s32[2]{0:T(128)S(1)}, s32[2]{0:T(128)}, u32[]{:S(2)}) copy-start(s32[2]{0:T(128)} %constant.199) | copy-start | bytes 28
  18.4 59.0 %copy-start.2 = (s32[2]{0:T(128)S(1)}, s32[2]{0:T(128)}, u32[]{:S(2)}) copy-start(s32[2]{0:T(128)} %constant.200) | copy-start | bytes 28
  59.8 1.3 collective-permute-start
  61.1 3.9 %collective-permute-start.1 = (f32[64,4,16]{0,2,1:T(8,128)S(1)}, f32[64,4,16]{0,2,1:T(8,128)S(1)}, u32[]{:S(2)}, u32[]{:S(2)}) collective-permute-start(f32[64,4,16]{0,2,1:T(8,128)S(1)} %add.56), channel_id=1, source_target_pairs={{0,2},{1,3},{2,0},{3,1},{4,6},{5,7},{6,4},{7,5},{8,10},{9,11},{10,... | collective-permute-start | bytes 49160 | tf_op jit(solution)/shard_map/ppermute | solution.py:48
  65.0 12.1 %collective-permute-start.2 = (f32[64,4,16]{0,2,1:T(8,128)S(1)}, f32[64,4,16]{0,2,1:T(8,128)S(1)}, u32[]{:S(2)}, u32[]{:S(2)}) collective-permute-start(f32[64,4,16]{0,2,1:T(8,128)S(1)} %add.57), channel_id=1, source_target_pairs={{0,4},{1,5},{2,6},{3,7},{4,0},{5,1},{6,2},{7,3},{8,12},{9,13},{10,... | collective-permute-start | bytes 49160 | tf_op jit(solution)/shard_map/ppermute | solution.py:48
  92.8 3.5 %copy-start = (bf16[16384,128]{1,0:T(8,128)(2,1)S(1)}, bf16[16384,128]{1,0:T(8,128)(2,1)}, u32[]{:S(2)}) copy-start(bf16[16384,128]{1,0:T(8,128)(2,1)} %get-tuple-element.205) | copy-start | bytes 12582916 | tf_op jit(solution)/shard_map/while
  112.7 3.5 %copy-start = (bf16[16384,128]{1,0:T(8,128)(2,1)S(1)}, bf16[16384,128]{1,0:T(8,128)(2,1)}, u32[]{:S(2)}) copy-start(bf16[16384,128]{1,0:T(8,128)(2,1)} %get-tuple-element.205) | copy-start | bytes 12582916 | tf_op jit(solution)/shard_map/while
